TPU v7x, 32 devices: a whole 2x2x4 slice. The times are simulated.
32 devices in a mesh: grp: 2 (over y), sp: 4 (over z), tp: 4 (over x, core).
Axes of the slice: x: 2, y: 2, z: 4, core: 2. Of those that a mesh axis runs over, the one named last changes fastest.
Arguments:
- tokens: bfloat16 [3072, 2048], P(('grp', 'sp'), 'tp'), parts along dimension 0, may hold values from -6 to 6
- norm_gain: float32 [2048], replicated, may hold values from 0.1 to 1.9
- qk_gain: float32 [4, 64], replicated, may hold values from 0.7 to 5.5
- w_query_window: bfloat16 [2048, 1024], P('sp', 'tp'), may hold values from -1 to 1
- w_key_window: bfloat16 [2048, 512], P('sp', 'tp'), may hold values from -1 to 1
- w_value_window: bfloat16 [2048, 512], P('sp', 'tp'), may hold values from -0.125 to 0.125
- sink_logits: float32 [16], P('tp'), may hold values from 0 to 5
- w_query_forget: bfloat16 [2048, 1024], P('sp', 'tp'), may hold values from -1 to 1
- w_key_forget: bfloat16 [2048, 1024], P('sp', 'tp'), may hold values from -1 to 1
- w_value_forget: bfloat16 [2048, 1024], P('sp', 'tp'), may hold values from -0.125 to 0.125
- gate_cum: float32 [3072, 16], P(('grp', 'sp'), 'tp'), parts along dimension 0, as said below
- w_merge: bfloat16 [2048, 2, 2048], P('sp', None, 'tp'), may hold values from -0.125 to 0.125
- w_branch: bfloat16 [2, 1024, 2048], P(None, 'sp', 'tp'), may hold values from -0.8984375 to 0.8984375
Outputs:
- mixed: bfloat16 [3072, 2048], P(('grp', 'sp'), 'tp'), parts along dimension 0
There are 2 independent parts, one for each index of `grp`. A program takes and returns all parts, laid end to end along the dimension named above; an argument that names none is the same for every part. Nothing has to cross between parts.
Inputs may be any that keep to these rules, and one draw needn't show every extreme that they name: `gate_cum`: along positions each head's values never rise.
All inputs are finite; a program needn't handle non-finite values.
Results may differ from a plain program's by a relative error of at most 0.012.
Values may be sent and summed in bfloat16 or wider, within the bound.
A program may use at most 64 MiB of HBM per device.

v0:
```python
import math

import jax
import jax.numpy as jnp
from jax import lax
from jax.sharding import PartitionSpec as P

HEAD = 64
WINDOW = 128


epsilon = 1e-06
big_negative = -1e30


def from_behind(value, axis, by):
    size = lax.axis_size(axis)
    pairs = [(i, i + by) for i in range(size) if 0 <= i + by < size]
    return lax.ppermute(value, axis, pairs)


def head_norm(raw, gain, head_count):
    split = raw.reshape(raw.shape[0], head_count, -1)
    scaled = split * lax.rsqrt(jnp.mean(split * split, axis=-1, keepdims=True) + epsilon) * gain
    return scaled.astype(jnp.bfloat16)


def window_attend(queries, keys_ext, values_ext, sink_rows, first_pos):
    row_count, head_count, head_size = queries.shape
    group_count = keys_ext.shape[1]
    span_rows = WINDOW // 2
    block_count = row_count // span_rows
    query_blocks = queries.reshape(
        block_count, span_rows, group_count, head_count // group_count, head_size
    )
    key_blocks = jnp.concatenate(
        [
            keys_ext[lag_index * span_rows : lag_index * span_rows + row_count].reshape(
                block_count, span_rows, group_count, head_size
            )
            for lag_index in range(3)
        ],
        axis=1,
    )
    value_blocks = jnp.concatenate(
        [
            values_ext[lag_index * span_rows : lag_index * span_rows + row_count].reshape(
                block_count, span_rows, group_count, head_size
            )
            for lag_index in range(3)
        ],
        axis=1,
    )
    scores = jnp.einsum(
        "nqgrd,nkgd->ngrqk", query_blocks, key_blocks, preferred_element_type=jnp.float32
    ) * head_size ** (-0.5)
    distance = WINDOW + jnp.arange(span_rows)[:, None] - jnp.arange(3 * span_rows)[None, :]
    key_pos = (
        first_pos
        - WINDOW
        + jnp.arange(block_count)[:, None] * span_rows
        + jnp.arange(3 * span_rows)[None, :]
    )
    is_valid = ((distance >= 0) & (distance < WINDOW))[None] & (key_pos >= 0)[:, None, :]
    is_valid = is_valid[:, None, None]
    sink_grid = sink_rows.reshape(1, group_count, head_count // group_count, 1)
    row_max = jnp.maximum(jnp.max(jnp.where(is_valid, scores, big_negative), axis=-1), sink_grid)
    weights = jnp.where(is_valid, jnp.exp(scores - row_max[..., None]), 0.0)
    row_total = jnp.sum(weights, axis=-1) + jnp.exp(sink_grid - row_max)
    prob_rows = (weights / row_total[..., None]).astype(jnp.bfloat16)
    mixed_sum = jnp.einsum(
        "ngrqk,nkgd->nqgrd", prob_rows, value_blocks, preferred_element_type=jnp.float32
    )
    return mixed_sum.reshape(row_count, head_count * head_size).astype(jnp.bfloat16)


def forget_groups(groups, keys, values, gates):
    head_count, head_size = (keys.shape[1], keys.shape[2])
    gates_all = lax.all_gather(gates, "sp", axis=0, tiled=True)

    def absorber(queries, query_gate, query_pos):

        def absorb(running, block):
            row_max, row_total, mixed_sum = running
            key_rows, value_rows, key_gate, key_pos = block
            scores = jnp.einsum(
                "qhd,khd->hqk", queries, key_rows, preferred_element_type=jnp.float32
            ) * head_size ** (-0.5)
            scores = scores + query_gate.T[:, :, None] - key_gate.T[:, None, :]
            is_valid = (query_pos[:, None] >= key_pos[None, :])[None]
            new_max = jnp.maximum(
                row_max, jnp.max(jnp.where(is_valid, scores, big_negative), axis=-1)
            )
            weights = jnp.where(is_valid, jnp.exp(scores - new_max[..., None]), 0.0)
            shrink = jnp.exp(row_max - new_max)
            row_total = row_total * shrink + jnp.sum(weights, axis=-1)
            mixed_sum = mixed_sum * shrink.T[:, :, None] + jnp.einsum(
                "hqk,khd->qhd",
                weights.astype(jnp.bfloat16),
                value_rows,
                preferred_element_type=jnp.float32,
            )
            return ((new_max, row_total, mixed_sum), None)

        return absorb

    initial = tuple(
        (
            (
                jnp.full((head_count, group[0].shape[0]), big_negative, jnp.float32),
                jnp.zeros((head_count, group[0].shape[0]), jnp.float32),
                jnp.zeros((group[0].shape[0], head_count, head_size), jnp.float32),
            )
            for group in groups
        )
    )
    first_row = jnp.int32(0)
    key_rows = lax.all_gather(keys, "sp", axis=0, tiled=True)
    value_rows = lax.all_gather(values, "sp", axis=0, tiled=True)
    piece_rows = key_rows.shape[0]
    sub_rows = math.gcd(piece_rows, 2048)
    turns = piece_rows // sub_rows
    key_gate = gates_all
    key_pos = jnp.arange(piece_rows)
    blocks = (
        key_rows.reshape(turns, sub_rows, head_count, head_size),
        value_rows.reshape(turns, sub_rows, head_count, head_size),
        key_gate.reshape(turns, sub_rows, head_count),
        key_pos.reshape(turns, sub_rows),
    )
    updated = []
    for (queries, query_gate, query_pos), state in zip(groups, initial):
        absorb = absorber(queries, query_gate, query_pos)

        def advance(current):
            return lax.scan(absorb, current, blocks)[0]

        def keep(current):
            return current

        updated.append(lax.cond(first_row <= query_pos[-1], advance, keep, state))
    finals = tuple(updated)
    return [
        (mixed_sum / row_total.T[:, :, None])
        .reshape(mixed_sum.shape[0], head_count * head_size)
        .astype(jnp.bfloat16)
        for row_max, row_total, mixed_sum in finals
    ]


def on_device(
    tokens,
    norm_gain,
    qk_gain,
    w_query_window,
    w_key_window,
    w_value_window,
    sink_logits,
    w_query_forget,
    w_key_forget,
    w_value_forget,
    gate_cum,
    w_merge,
    w_branch,
):
    row_count = tokens.shape[0]
    row_offset = lax.axis_index("sp") * row_count
    gathered = lax.all_gather(tokens, "tp", axis=1, tiled=True)
    as_float = gathered.astype(jnp.float32)
    normed = (
        as_float
        * lax.rsqrt(jnp.mean(as_float * as_float, axis=-1, keepdims=True) + epsilon)
        * norm_gain
    ).astype(jnp.bfloat16)
    merge_flat = w_merge.reshape(w_merge.shape[0], -1)
    pieces = (
        lax.all_gather(w_query_window, "sp", axis=0, tiled=True),
        lax.all_gather(w_key_window, "sp", axis=0, tiled=True),
        lax.all_gather(w_value_window, "sp", axis=0, tiled=True),
        lax.all_gather(w_query_forget, "sp", axis=0, tiled=True),
        lax.all_gather(w_key_forget, "sp", axis=0, tiled=True),
        lax.all_gather(w_value_forget, "sp", axis=0, tiled=True),
        lax.all_gather(merge_flat, "sp", axis=0, tiled=True),
    )
    projected = tuple(
        (jnp.dot(normed, weight_rows, preferred_element_type=jnp.float32) for weight_rows in pieces)
    )
    query_heads = w_query_window.shape[1] // HEAD
    group_heads = w_key_window.shape[1] // HEAD
    window_query = head_norm(projected[0], qk_gain[0], query_heads)
    window_key = head_norm(projected[1], qk_gain[1], group_heads)
    window_value = projected[2].astype(jnp.bfloat16).reshape(row_count, group_heads, HEAD)
    prev_key, prev_value = from_behind(
        (window_key[row_count - WINDOW :], window_value[row_count - WINDOW :]), "sp", 1
    )
    window_out = window_attend(
        window_query,
        jnp.concatenate([prev_key, window_key], axis=0),
        jnp.concatenate([prev_value, window_value], axis=0),
        sink_logits,
        row_offset,
    )
    forget_query = head_norm(projected[3], qk_gain[2], query_heads)
    forget_key = head_norm(projected[4], qk_gain[3], query_heads)
    forget_value = projected[5].astype(jnp.bfloat16).reshape(row_count, query_heads, HEAD)
    own_pos = row_offset + jnp.arange(row_count)
    forget_out = forget_groups(
        [(forget_query, gate_cum, own_pos)], forget_key, forget_value, gate_cum
    )[0]
    channel_count = w_merge.shape[2]
    merge_gate = jax.nn.sigmoid(projected[6]).reshape(row_count, 2, channel_count)
    branch_full = lax.all_gather(w_branch, "sp", axis=1, tiled=True)
    head_stack = jnp.stack([window_out, forget_out], axis=1)
    weight_rows = branch_full
    projection = jnp.einsum(
        "uxa,xag->uxg",
        lax.all_gather(head_stack, "tp", axis=2, tiled=True),
        weight_rows,
        preferred_element_type=jnp.float32,
    )
    return (merge_gate[:, 0] * projection[:, 0] + merge_gate[:, 1] * projection[:, 1]).astype(
        jnp.bfloat16
    )


def solution(mesh):
    return jax.shard_map(
        on_device,
        mesh=mesh,
        in_specs=(
            P(("grp", "sp"), "tp"),
            P(),
            P(),
            P("sp", "tp"),
            P("sp", "tp"),
            P("sp", "tp"),
            P("tp"),
            P("sp", "tp"),
            P("sp", "tp"),
            P("sp", "tp"),
            P(("grp", "sp"), "tp"),
            P("sp", None, "tp"),
            P(None, "sp", "tp"),
        ),
        out_specs=P(("grp", "sp"), "tp"),
        check_vma=False,
    )
```

profile of v0, /device:TPU:24, one launch (start us, length us, event | category | flops | bytes accessed | tf_op | source)
XLA Modules:
  0.0 335.1 jit_solution(14842164746860835694)
XLA Ops:
  11.2 1.3 slice.58
  13.7 14.0 %all_gather.48 = f32[1536,4]{0,1:T(4,128)} all-gather(f32[384,4]{0,1:T(4,128)} %param.27), channel_id=1, replica_groups=mesh['grp'=2,'sp'=4,'tp'=4] {'sp'}, dimensions={0}, use_global_device_ids=true | all-gather | bytes 30720 | tf_op jit(solution)/shard_map/all_gather | solution.py:79
  27.9 19.2 %all_gather.42 = bf16[2048,128]{1,0:T(8,128)(2,1)} all-gather(bf16[512,128]{1,0:T(8,128)(2,1)S(1)} %copy-done.8), channel_id=1, replica_groups=mesh['grp'=2,'sp'=4,'tp'=4] {'sp'}, dimensions={0}, use_global_device_ids=true | all-gather | bytes 655360 | tf_op jit(solution)/shard_map/all_gather | solution.py:178
  47.8 20.2 %all_gather.41 = bf16[2048,128]{1,0:T(8,128)(2,1)} all-gather(bf16[512,128]{1,0:T(8,128)(2,1)S(1)} %copy-done.9), channel_id=1, replica_groups=mesh['grp'=2,'sp'=4,'tp'=4] {'sp'}, dimensions={0}, use_global_device_ids=true | all-gather | bytes 655360 | tf_op jit(solution)/shard_map/all_gather | solution.py:179
  68.7 1.9 fusion.25
  71.1 2.5 multiply_reduce_fusion.1
  73.8 27.6 %all_gather.45 = bf16[1536,4,64]{0,2,1:T(8,128)(2,1)S(1)} all-gather(bf16[384,4,64]{0,2,1:T(8,128)(2,1)S(1)} %multiply_convert_fusion.2), channel_id=1, replica_groups=mesh['grp'=2,'sp'=4,'tp'=4] {'sp'}, dimensions={0}, use_global_device_ids=true | all-gather | bytes 983040 | tf_op jit(solution)/shard_map/all_gather | solution.py:118
  101.3 3.0 all-gather.17.cloned.1.call-done
  104.4 2.0 convolution_convert_fusion.1
  106.3 27.7 %all_gather.47 = bf16[1536,4,64]{0,2,1:T(8,128)(2,1)S(1)} all-gather(bf16[384,4,64]{0,2,1:T(8,128)(2,1)S(1)} %bitcast.165), channel_id=1, replica_groups=mesh['grp'=2,'sp'=4,'tp'=4] {'sp'}, dimensions={0}, use_global_device_ids=true | all-gather | bytes 983040 | tf_op jit(solution)/shard_map/all_gather | solution.py:119
  134.1 6.1 %all-gather.19.cloned.1.call-done = bf16[2048,256]{1,0:T(8,128)(2,1)} async-done(((bf16[512,256]{1,0:T(8,128)(2,1)}), bf16[2048,256]{1,0:T(8,128)(2,1)}) %all-gather.19.cloned.1.call-update) | async-done | bytes 1048592 | tf_op jit(solution)/shard_map/all_gather | solution.py:180
  140.1 2.1 multiply_reduce_fusion
  142.2 1.2 multiply_reduce_fusion.2
  143.4 1.2 convolution_convert_fusion.2
  145.5 35.6 %conditional.1 = (f32[4,384]{1,0:T(4,128)}, f32[384,4,64]{0,2,1:T(8,128)}) conditional(s32[]{:T(128)} %bitcast.13, () %tuple.20, (bf16[1536,4,64]{0,2,1:T(8,128)(2,1)S(1)}, bf16[1536,4,64]{0,2,1:T(8,128)(2,1)S(1)}, f32[1536,4]{0,1:T(4,128)}, s32[3,512]{1,0:T(4,128)S(1)}, s32[3,512]{1,0:T(4,128)S(1)}, /*index=5*/s32[384]{0:T(512)}, ...), branch_computations={%region_7.8_spmd, %region_8.13_spmd} | conditional | flops 215199744 | bytes 15060769 | solution.py:141
  146.1 1.4 copy_bitcast_fusion
  147.4 33.6 %while.18 = (s32[]{:T(128)}, f32[4,384]{1,0:T(4,128)S(1)}, f32[4,384]{1,0:T(4,128)}, f32[384,4,64]{0,2,1:T(8,128)}, s32[384]{0:T(512)}, /*index=5*/s32[3,512]{1,...) while((s32[]{:T(128)}, f32[4,384]{1,0:T(4,128)S(1)}, ...), condition=%wide.region_12.12_spmd.clone, body=%wide.region_9.11_spmd.clone.sunk | while | flops 215196672 | bytes 11896481 | solution.py:136
  148.8 0.9 broadcast_compare_fusion.2
  149.7 2.7 fusion.85
  153.1 1.6 fusion.87
  155.3 2.7 fusion.89
  159.5 0.9 broadcast_compare_fusion.2
  160.3 2.7 fusion.85
  163.7 1.6 fusion.87
  165.3 1.3 fusion.88
  166.6 2.9 fusion.89
  170.9 0.9 broadcast_compare_fusion.2
  171.8 2.7 fusion.85
  175.1 1.6 fusion.87
  176.8 1.3 fusion.88
  178.1 2.9 fusion.89
  181.0 1.0 divide_convert_fusion.2
  182.1 2.5 bitcast_reduce_fusion
  186.3 1.3 collective-permute-start.1
  187.6 1.5 collective-permute-start
  189.1 1.0 multiply_convert_fusion
  190.2 3.4 %collective-permute-done.1 = bf16[128,2,64]{0,2,1:T(8,128)(2,1)S(1)} collective-permute-done((bf16[128,2,64]{0,2,1:T(8,128)(2,1)S(1)}, bf16[128,2,64]{0,2,1:T(8,128)(2,1)S(1)}, u32[]{:S(2)}, u32[]{:S(2)}) %collective-permute-start.1) | collective-permute-done | bytes 32800 | tf_op jit(solution)/shard_map/ppermute | solution.py:19
  194.2 1.9 collective-permute-done
  198.1 1.0 fusion.32
  200.6 1.3 copy.55
  201.9 14.3 %all-gather.23.cloned.1.call-done = bf16[2,1024,512]{2,1,0:T(8,128)(2,1)} async-done(((bf16[2,256,512]{2,1,0:T(8,128)(2,1)}), bf16[2,1024,512]{2,1,0:T(8,128)(2,1)}) %all-gather.23.cloned.1.call-update) | async-done | bytes 2097168 | tf_op jit(solution)/shard_map/all_gather | solution.py:212
  216.3 22.2 %all-gather.21.cloned.1.call-done = bf16[384,2,1024]{2,0,1:T(8,128)(2,1)} async-done(((bf16[384,2,256]{2,0,1:T(8,128)(2,1)}), bf16[384,2,1024]{2,0,1:T(8,128)(2,1)}) %all-gather.21.cloned.1.call-update) | async-done | bytes 1572880 | tf_op jit(solution)/shard_map/all_gather | solution.py:217
  238.4 3.0 convolution_bitcast_fusion
  241.5 76.6 %all-gather.11.cloned.1.call-done = bf16[2048,1024]{1,0:T(8,128)(2,1)} async-done(((bf16[512,1024]{1,0:T(8,128)(2,1)}), bf16[2048,1024]{1,0:T(8,128)(2,1)}) %all-gather.11.cloned.1.call-update) | async-done | bytes 4194320 | tf_op jit(solution)/shard_map/all_gather | solution.py:183
  318.0 5.3 %add_divide_fusion = f32[384,1024]{1,0:T(8,128)} fusion(bf16[384,2048]{1,0:T(8,128)(2,1)S(1)} %copy-done.1, bf16[2048,1024]{1,0:T(8,128)(2,1)} %all-gather.11.cloned.1.call-done), kind=kOutput, calls=%fused_computation.44 | convolution fusion | flops 1611792384 | bytes 7340032 | tf_op jit(solution)/shard_map/dot_general | solution.py:186
  323.3 2.6 reshape.258
  326.0 1.2 fusion.56
  327.2 1.0 fusion.36
  (119 shorter events, 21.2 us)
Async XLA Ops:
  6.5 6.6 %copy-start.15 = (f32[4,64]{1,0:T(4,128)S(1)}, f32[4,64]{1,0:T(4,128)}, u32[]{:S(2)}) copy-start(f32[4,64]{1,0:T(4,128)} %param.19) | copy-start | bytes 3076
  6.5 21.3 %copy-start.8 = (bf16[512,128]{1,0:T(8,128)(2,1)S(1)}, bf16[512,128]{1,0:T(8,128)(2,1)}, u32[]{:S(2)}) copy-start(bf16[512,128]{1,0:T(8,128)(2,1)} %param.21) | copy-start | bytes 393220
  6.5 40.5 %copy-start.16 = (f32[4]{0:T(128)S(1)}, f32[4]{0:T(128)}, u32[]{:S(2)}) copy-start(f32[4]{0:T(128)} %param.23) | copy-start | bytes 52
  6.5 41.2 %copy-start.9 = (bf16[512,128]{1,0:T(8,128)(2,1)S(1)}, bf16[512,128]{1,0:T(8,128)(2,1)}, u32[]{:S(2)}) copy-start(bf16[512,128]{1,0:T(8,128)(2,1)} %param.22) | copy-start | bytes 393220
  6.5 62.1 %all-gather.9.cloned.1.call-start = ((), (), s32[]{:S(2)}) async-start(), calls=%async_computation | async-start | bytes 1966080 | tf_op jit(solution)/shard_map/all_gather | solution.py:168
  7.3 63.8 %all-gather.15.cloned.1.call-start = ((), (), s32[]{:S(2)}) async-start(), calls=%async_computation.3 | async-start | bytes 1310720 | tf_op jit(solution)/shard_map/all_gather | solution.py:181
  8.0 96.3 %all-gather.17.cloned.1.call-start = ((), (), s32[]{:S(2)}) async-start(), calls=%async_computation.4 | async-start | bytes 1310720 | tf_op jit(solution)/shard_map/all_gather | solution.py:182
  8.8 131.4 %all-gather.19.cloned.1.call-start = ((), (), s32[]{:S(2)}) async-start(), calls=%async_computation.5 | async-start | bytes 1310720 | tf_op jit(solution)/shard_map/all_gather | solution.py:180
  9.3 172.7 %all-gather.13.cloned.1.call-start = ((), (), s32[]{:S(2)}) async-start(), calls=%async_computation.2 | async-start | bytes 1310720 | tf_op jit(solution)/shard_map/all_gather | solution.py:177
  9.9 206.3 %all-gather.23.cloned.1.call-start = ((), (), s32[]{:S(2)}) async-start(), calls=%async_computation.7 | async-start | bytes 2621440 | tf_op jit(solution)/shard_map/all_gather | solution.py:212
  10.5 60.1 %copy-start.11 = (f32[2048]{0:T(1024)S(1)}, f32[2048]{0:T(1024)}, u32[]{:S(2)}) copy-start(f32[2048]{0:T(1024)} %param.18) | copy-start | bytes 24580
  10.5 227.9 %all-gather.21.cloned.1.call-start = ((), (), s32[]{:S(2)}) async-start(), calls=%async_computation.6 | async-start | bytes 1966080 | tf_op jit(solution)/shard_map/all_gather | solution.py:217
  68.7 1.9 copy-start.2
  71.1 72.4 %copy-start = (bf16[384,2048]{1,0:T(8,128)(2,1)}, bf16[384,2048]{1,0:T(8,128)(2,1)S(1)}, u32[]{:S(2)}) copy-start(bf16[384,2048]{1,0:T(8,128)(2,1)S(1)} %fusion.27) | copy-start | bytes 4718596
  140.1 2.1 copy-start.3
  142.2 1.2 copy-start.4
  182.0 2.6 copy-start.5
  184.9 1.1 copy-start.10
  185.0 1.2 copy-start.12
  185.1 4.0 %copy-start.14 = (f32[64]{0:T(128)S(1)}, f32[64]{0:T(128)}, u32[]{:S(2)}) copy-start(f32[64]{0:T(128)} %get-tuple-element.195) | copy-start | bytes 772
  186.3 7.4 %collective-permute-start.1 = (bf16[128,2,64]{0,2,1:T(8,128)(2,1)S(1)}, bf16[128,2,64]{0,2,1:T(8,128)(2,1)S(1)}, u32[]{:S(2)}, u32[]{:S(2)}) collective-permute-start(bf16[128,2,64]{0,2,1:T(8,128)(2,1)S(1)} %slice.68), channel_id=1, source_target_pairs={{0,4},{4,8},{8,12},{1,5},{5,9},{9,13},{2,6},{6,10},{10,14},{3,7},{... | collective-permute-start | bytes 98312 | tf_op jit(solution)/shard_map/ppermute | solution.py:19
  187.6 8.5 %collective-permute-start = (bf16[128,2,64]{0,2,1:T(8,128)(2,1)S(1)}, bf16[128,2,64]{0,2,1:T(8,128)(2,1)S(1)}, u32[]{:S(2)}, u32[]{:S(2)}) collective-permute-start(bf16[128,2,64]{0,2,1:T(8,128)(2,1)S(1)} %bitcast.167), channel_id=1, source_target_pairs={{0,4},{4,8},{8,12},{1,5},{5,9},{9,13},{2,6},{6,10},{10,14},{3,7},{... | collective-permute-start | bytes 98312 | tf_op jit(solution)/shard_map/ppermute | solution.py:19
  194.0 2.7 copy-start.7
  196.6 0.7 copy-start.13
  199.1 1.5 copy-start.6
  200.6 117.4 %all-gather.11.cloned.1.call-start = ((), (), s32[]{:S(2)}) async-start(), calls=%async_computation.1 | async-start | bytes 5242880 | tf_op jit(solution)/shard_map/all_gather | solution.py:183
  201.9 116.1 %copy-start.1 = (bf16[384,2048]{1,0:T(8,128)(2,1)S(1)}, bf16[384,2048]{1,0:T(8,128)(2,1)}, u32[]{:S(2)}) copy-start(bf16[384,2048]{1,0:T(8,128)(2,1)} %copy-done) | copy-start | bytes 4718596
Sparse Core Ops, SparseCore 0:
  8.9 20.5 all-gather.8
  31.1 35.9 all-gather.14
  68.7 35.5 all-gather.16
  105.8 34.3 all-gather.18
  141.6 27.2 all-gather.12
  170.3 45.9 all-gather.22
  217.8 20.5 all-gather.20
  240.0 77.9 all-gather.10
where the time goes:
time: 341 us; the launch traced here: 335 us
  waiting for transfers between devices  131 us (38%)
  blocking collectives  109 us (32%)
  matrix products  38 us (11%)
  other arithmetic  23.1 us (7%)
  local copies, waits for them, and re-layouts  16.3 us (5%)
  between operations  14.7 us (4%)
    all_gather x1, waiting for transfers between devices, on_device(): lax.all_gather(merge_flat, 'sp', axis=0, tiled=True)  76.6 us
    all_gather x1, blocking collectives, forget_groups(): value_rows = lax.all_gather(values, 'sp', axis=0, tiled=True)  27.7 us
    all_gather x1, blocking collectives, forget_groups(): key_rows = lax.all_gather(keys, 'sp', axis=0, tiled=True)  27.6 us
    all_gather x1, waiting for transfers between devices, on_device(): lax.all_gather(head_stack, 'tp', axis=2, tiled=True)  22.2 us
    all_gather x1, blocking collectives, on_device(): lax.all_gather(w_value_window, 'sp', axis=0, tiled=True)  20.2 us
    all_gather x1, blocking collectives, on_device(): lax.all_gather(w_key_window, 'sp', axis=0, tiled=True)  19.2 us
    dot_general x7, matrix products, on_device(): jnp.dot(normed, weight_rows, preferred_element_type=jnp.float32)  16.8 us
    all_gather x1, waiting for transfers between devices, on_device(): branch_full = lax.all_gather(w_branch, 'sp', axis=1, tiled=True)  14.3 us
  transfers between devices with their start and end apart: 10, of which 7 were waited for; matrix products, arithmetic and copies ran while one was open for 20% of the time, Pallas kernels for 0%

commit v1 on v0

v1 whole, which is shorter than its diff:
```python
import functools

import jax
import jax.numpy as jnp
from jax import lax
from jax.experimental import pallas as pl
from jax.experimental.pallas import tpu as pltpu
from jax.sharding import PartitionSpec as P

HEAD = 64
PAIR = 2 * HEAD
WINDOW = 128

epsilon = 1e-06
big_negative = -1e30
VMEM_LIMIT = 60 * 1024 * 1024


def from_behind(value, axis, by):
    size = lax.axis_size(axis)
    pairs = [(i, i + by) for i in range(size) if 0 <= i + by < size]
    return lax.ppermute(value, axis, pairs)


def project_kernel(sections, tokens_ref, gain_ref, weight_ref, head_gain_ref, normed_ref, *outs):
    x = tokens_ref[...].astype(jnp.float32)
    scale = lax.rsqrt(jnp.mean(x * x, axis=-1, keepdims=True) + epsilon)
    normed_ref[...] = (x * scale * gain_ref[...]).astype(jnp.bfloat16)
    low = lax.broadcasted_iota(jnp.int32, (1, PAIR), 1) < HEAD
    normed = normed_ref[...]
    start = 0
    for out_ref, flags in zip(outs, sections):
        width = out_ref.shape[1]
        raw = jnp.dot(normed, weight_ref[:, start : start + width], preferred_element_type=jnp.float32)
        for at in range(0, width, PAIR):
            part = raw[:, at : at + PAIR]
            first, second = flags[at // HEAD], flags[at // HEAD + 1]
            if first or second:
                squares = part * part
                lower = jnp.sum(jnp.where(low, squares, 0.0), axis=-1, keepdims=True)
                upper = jnp.sum(jnp.where(low, 0.0, squares), axis=-1, keepdims=True)
                factor = jnp.where(
                    low,
                    lax.rsqrt(lower * (1.0 / HEAD) + epsilon),
                    lax.rsqrt(upper * (1.0 / HEAD) + epsilon),
                )
                scaled = part * factor * head_gain_ref[:, start + at : start + at + PAIR]
                if first and second:
                    part = scaled
                else:
                    part = jnp.where(low if first else ~low, scaled, part)
            out_ref[:, at : at + PAIR] = part.astype(jnp.bfloat16)
        start += width


def attend_kernel(heads, q_ref, kv_ref, gates_ref, wkv_ref, sink_ref, out_ref):
    rows = q_ref.shape[0]
    width = heads * HEAD
    shard = lax.axis_index("sp")
    low = lax.broadcasted_iota(jnp.int32, (1, PAIR), 1) < HEAD
    contract = (((1,), (1,)), ((), ()))
    for pair in range(heads // 2):
        lanes = pair * PAIR
        queries = q_ref[:, width + lanes : width + lanes + PAIR] * jnp.bfloat16(HEAD ** -0.5)
        split = [jnp.where(low, queries, jnp.bfloat16(0)), jnp.where(low, jnp.bfloat16(0), queries)]
        diagonal = lax.broadcasted_iota(jnp.int32, (rows, rows), 0) >= lax.broadcasted_iota(
            jnp.int32, (rows, rows), 1
        )

        def block(index, carry, masked):
            at = pl.ds(pl.multiple_of(index * rows, rows), rows)
            keys = kv_ref[at, lanes : lanes + PAIR]
            values = kv_ref[at, width + lanes : width + lanes + PAIR]
            result = []
            for half in range(2):
                top, total, mixed = carry[half]
                head = pair * 2 + half
                scores = lax.dot_general(split[half], keys, contract, preferred_element_type=jnp.float32)
                scores = scores - gates_ref[index, head : head + 1, :]
                if masked:
                    scores = jnp.where(diagonal, scores, big_negative)
                new_top = jnp.maximum(top, jnp.max(scores, axis=-1, keepdims=True))
                weights = jnp.exp(scores - new_top)
                if masked:
                    weights = jnp.where(diagonal, weights, 0.0)
                shrink = jnp.exp(top - new_top)
                total = total * shrink + jnp.sum(weights, axis=-1, keepdims=True)
                mixed = mixed * shrink + jnp.dot(
                    weights.astype(jnp.bfloat16), values, preferred_element_type=jnp.float32
                )
                result.append((new_top, total, mixed))
            return tuple(result)

        empty = (
            jnp.full((rows, 1), big_negative, jnp.float32),
            jnp.zeros((rows, 1), jnp.float32),
            jnp.zeros((rows, PAIR), jnp.float32),
        )
        state = block(shard, (empty, empty), True)
        state = lax.fori_loop(0, shard, lambda i, c: block(i, c, False), state)
        mixed = jnp.where(low, state[0][2] / state[0][1], state[1][2] / state[1][1])
        out_ref[:, width + lanes : width + lanes + PAIR] = mixed.astype(jnp.bfloat16)

        keys = wkv_ref[:, pair * HEAD : (pair + 1) * HEAD]
        values = wkv_ref[:, width // 2 + pair * HEAD : width // 2 + (pair + 1) * HEAD]
        keys = jnp.concatenate([keys, keys], axis=1)
        values = jnp.concatenate([values, values], axis=1)
        row_at = lax.broadcasted_iota(jnp.int32, (WINDOW, 2 * WINDOW), 0)
        col_at = lax.broadcasted_iota(jnp.int32, (WINDOW, 2 * WINDOW), 1)
        inside = (col_at > row_at) & (col_at <= row_at + WINDOW)
        for at in range(0, rows, WINDOW):
            queries = q_ref[at : at + WINDOW, lanes : lanes + PAIR] * jnp.bfloat16(HEAD ** -0.5)
            near = keys[at : at + 2 * WINDOW]
            near_values = values[at : at + 2 * WINDOW]
            valid = inside
            if at == 0:
                valid = inside & ((col_at >= WINDOW) | (shard > 0))
            parts = []
            for half in range(2):
                head = pair * 2 + half
                mine = jnp.where(low if half == 0 else ~low, queries, jnp.bfloat16(0))
                scores = lax.dot_general(mine, near, contract, preferred_element_type=jnp.float32)
                sink = sink_ref[:, head : head + 1]
                top = jnp.maximum(
                    jnp.max(jnp.where(valid, scores, big_negative), axis=-1, keepdims=True), sink
                )
                weights = jnp.where(valid, jnp.exp(scores - top), 0.0)
                total = jnp.sum(weights, axis=-1, keepdims=True) + jnp.exp(sink - top)
                probs = (weights / total).astype(jnp.bfloat16)
                parts.append(jnp.dot(probs, near_values, preferred_element_type=jnp.float32))
            out_ref[at : at + WINDOW, lanes : lanes + PAIR] = jnp.where(low, parts[0], parts[1]).astype(
                jnp.bfloat16
            )


def gather_rows(shard):
    parts = lax.axis_size("grp")
    rows = shard.shape[0] // parts
    mine = lax.dynamic_slice_in_dim(shard, lax.axis_index("grp") * rows, rows, axis=0)
    return lax.all_gather(mine, ("sp", "grp"), axis=0, tiled=True)


def on_device(
    tokens,
    norm_gain,
    qk_gain,
    w_query_window,
    w_key_window,
    w_value_window,
    sink_logits,
    w_query_forget,
    w_key_forget,
    w_value_forget,
    gate_cum,
    w_merge,
    w_branch,
):
    rows = tokens.shape[0]
    shards = lax.axis_size("sp")
    heads = w_query_window.shape[1] // HEAD
    groups = w_key_window.shape[1] // HEAD
    channels = w_merge.shape[2]
    gathered = lax.all_gather(tokens, "tp", axis=1, tiled=True)
    weights = gather_rows(
        jnp.concatenate(
            [w_query_window, w_query_forget, w_key_forget, w_value_forget, w_key_window, w_value_window],
            axis=1,
        )
    )
    head_gains = jnp.concatenate(
        [
            jnp.tile(qk_gain[0], heads),
            jnp.tile(qk_gain[2], heads),
            jnp.tile(qk_gain[3], heads),
            jnp.ones((heads * HEAD,), jnp.float32),
            jnp.tile(qk_gain[1], groups),
            jnp.ones((groups * HEAD,), jnp.float32),
        ]
    )[None]
    sections = (
        (True,) * (2 * heads),
        (True,) * heads + (False,) * heads,
        (True,) * groups + (False,) * groups,
    )
    depth = gathered.shape[1]
    normed, queries, forget_kv, window_kv = pl.pallas_call(
        functools.partial(project_kernel, sections),
        out_shape=(
            jax.ShapeDtypeStruct((rows, depth), jnp.bfloat16),
            *(jax.ShapeDtypeStruct((rows, len(s) * HEAD), jnp.bfloat16) for s in sections),
        ),
        compiler_params=pltpu.CompilerParams(vmem_limit_bytes=VMEM_LIMIT),
        cost_estimate=pl.CostEstimate(
            flops=2 * rows * depth * weights.shape[1], bytes_accessed=8 * 1024 * 1024, transcendentals=0
        ),
        name="project",
    )(gathered, norm_gain[None], weights, head_gains)
    behind = from_behind(window_kv[rows - WINDOW :], "sp", 1)
    kv_all = lax.all_gather(forget_kv, "sp", axis=0, tiled=True)
    gates_all = lax.all_gather(gate_cum.T, "sp", axis=0)
    attended = pl.pallas_call(
        functools.partial(attend_kernel, heads),
        out_shape=jax.ShapeDtypeStruct((rows, 2 * heads * HEAD), jnp.bfloat16),
        compiler_params=pltpu.CompilerParams(vmem_limit_bytes=VMEM_LIMIT),
        cost_estimate=pl.CostEstimate(
            flops=8 * rows * rows * shards * heads * HEAD,
            bytes_accessed=4 * 1024 * 1024,
            transcendentals=rows * rows * shards * heads,
        ),
        name="attend",
    )(queries, kv_all, gates_all, jnp.concatenate([behind, window_kv], axis=0), sink_logits[None])
    merge_rows = gather_rows(w_merge.reshape(w_merge.shape[0], -1))
    merge_gate = jax.nn.sigmoid(jnp.dot(normed, merge_rows, preferred_element_type=jnp.float32))
    branch_full = gather_rows(w_branch.swapaxes(0, 1)).swapaxes(0, 1)
    width = heads * HEAD
    head_all = lax.all_gather(attended.reshape(rows, 2, width), "tp", axis=2, tiled=True)
    window_projection = jnp.dot(head_all[:, 0], branch_full[0], preferred_element_type=jnp.float32)
    forget_projection = jnp.dot(head_all[:, 1], branch_full[1], preferred_element_type=jnp.float32)
    return (
        merge_gate[:, :channels] * window_projection + merge_gate[:, channels:] * forget_projection
    ).astype(jnp.bfloat16)


def solution(mesh):
    return jax.shard_map(
        on_device,
        mesh=mesh,
        in_specs=(
            P(("grp", "sp"), "tp"),
            P(),
            P(),
            P("sp", "tp"),
            P("sp", "tp"),
            P("sp", "tp"),
            P("tp"),
            P("sp", "tp"),
            P("sp", "tp"),
            P("sp", "tp"),
            P(("grp", "sp"), "tp"),
            P("sp", None, "tp"),
            P(None, "sp", "tp"),
        ),
        out_specs=P(("grp", "sp"), "tp"),
        check_vma=False,
    )
```

time: 341 us -> 316 us (0.927); the launches traced: 335 us -> 314 us
  waiting for transfers between devices: 131 us -> 245 us
  blocking collectives: 109 us -> 15.4 us
  matrix products: 38 us -> 9.26 us
  other arithmetic: 23.1 us -> 0.73 us
  Pallas kernels: 0 us -> 21.2 us
  local copies, waits for them, and re-layouts: 16.3 us -> 7.56 us
    all_gather x7 -> x5, waiting for transfers between devices: 122 us -> 226 us  [the longest x3 189 us: gather_rows(): return lax.all_gather(mine, ('sp', 'grp'), axis=0, tiled=True)]
    all_gather x5 -> x1, blocking collectives: 109 us -> 15.4 us  [on_device(): gates_all = lax.all_gather(gate_cum.T, 'sp', axis=0)]
    dot_general x16 -> x3, matrix products: 38 us -> 9.26 us  [the longest x1 4.6 us: on_device(): jnp.dot(normed, merge_rows, preferred_element_type=jnp.float32)]
    pallas_call x0 -> x2, Pallas kernels: none -> 21.2 us  [the longest x1 14.8 us: on_device(): pl.pallas_call(functools.partial(attend_kernel, heads), out_shape=jax.Sha...]
    all_gather x1, waiting for transfers between devices: 0.01 us -> 18.1 us  [on_device(): gathered = lax.all_gather(tokens, 'tp', axis=1, tiled=True)]
    reduce_sum x5 -> x0, other arithmetic: 7.41 us -> none  [the longest x3 4.88 us: absorb(): row_total = row_total * shrink + jnp.sum(weights, axis=-1)]
    ppermute x2 -> x1, waiting for transfers between devices: 5.32 us -> 0.01 us  [from_behind(): return lax.ppermute(value, axis, pairs)]
    convert_element_type x8 -> x0, other arithmetic: 4.54 us -> none  [the longest x5 2.04 us: head_norm(): return scaled.astype(jnp.bfloat16)]
  transfers between devices with their start and end apart: 10 -> 7, of which waited for: 7 -> 6; matrix products, arithmetic and copies ran while one was open for 20% -> 4% of each run, Pallas kernels for 0% -> 5%
where the time goes in v1:
time: 316 us; the launch traced here: 314 us
  waiting for transfers between devices  245 us (78%)
  Pallas kernels  21.2 us (7%)
  blocking collectives  15.4 us (5%)
  between operations  13.7 us (4%)
  matrix products  9.26 us (3%)
  local copies, waits for them, and re-layouts  7.56 us (2%)
    all_gather x3, waiting for transfers between devices, gather_rows(): return lax.all_gather(mine, ('sp', 'grp'), axis=0, tiled=True)  189 us
    all_gather x1, waiting for transfers between devices, on_device(): lax.all_gather(attended.reshape(rows, 2, width), 'tp', axis=2, tiled=True)  21.3 us
    all_gather x1, waiting for transfers between devices, on_device(): gathered = lax.all_gather(tokens, 'tp', axis=1, tiled=True)  18.1 us
    all_gather x1, waiting for transfers between devices, on_device(): kv_all = lax.all_gather(forget_kv, 'sp', axis=0, tiled=True)  15.9 us
    all_gather x1, blocking collectives, on_device(): gates_all = lax.all_gather(gate_cum.T, 'sp', axis=0)  15.4 us
    pallas_call x1, Pallas kernels, on_device(): pl.pallas_call(functools.partial(attend_kernel, heads), out_shape=jax.Sha...  14.8 us
    pallas_call x1, Pallas kernels, on_device(): pl.pallas_call(functools.partial(project_kernel, sections), out_shape=(ja...  6.42 us
  transfers between devices with their start and end apart: 7, of which 6 were waited for; matrix products, arithmetic and copies ran while one was open for 4% of the time, Pallas kernels for 5%

profile of v1, /device:TPU:24, one launch (start us, length us, event | category | flops | bytes accessed | tf_op | source)
XLA Modules:
  0.0 314.4 jit_solution(7647228694275138529)
XLA Ops:
  6.5 0.0 copy-start
  6.5 0.0 all-gather.9.cloned.1.call-start
  6.6 0.7 all-gather.9.cloned.1.call-update
  7.3 0.0 all-gather.11.cloned.1.call-start
  7.3 1.0 constant_dynamic-update-slice_fusion.5
  8.3 1.0 constant_dynamic-update-slice_fusion.4
  9.3 0.0 copy-done.3
  9.3 0.0 copy-done.4
  9.3 0.0 copy-start.8
  9.4 0.0 copy-done.5
  9.4 0.0 copy-done.6
  9.5 0.9 constant_dynamic-slice_fusion.1
  10.4 0.0 all-gather.11.cloned.1.call-update
  10.4 0.0 all-gather.15.cloned.1.call-start
  10.4 0.0 copy-done.8
  10.5 0.1 tile.42
  10.6 0.1 tile.45
  10.7 0.1 tile.48
  10.7 0.1 tile.51
  10.9 0.6 broadcast_in_dim.18.head_gain_ref
  11.5 18.1 %all-gather.9.cloned.1.call-done.tokens_ref = bf16[384,2048]{1,0:T(8,128)(2,1)} async-done(((bf16[384,512]{1,0:T(8,128)(2,1)}), bf16[384,2048]{1,0:T(8,128)(2,1)}) %all-gather.9.cloned.1.call-update) | async-done | bytes 1572880 | tf_op jit(solution)/shard_map/all_gather | solution.py:163
  29.6 86.3 %all-gather.11.cloned.1.call-done.weight_ref = bf16[2048,1280]{1,0:T(8,128)(2,1)} async-done(((bf16[256,1280]{1,0:T(8,128)(2,1)}), bf16[2048,1280]{1,0:T(8,128)(2,1)}) %all-gather.11.cloned.1.call-update) | async-done | bytes 5242896 | tf_op jit(solution)/shard_map/all_gather | solution.py:140
  115.8 6.4 %project.1 = (bf16[384,2048]{1,0:T(8,128)(2,1)}, bf16[384,512]{1,0:T(8,128)(2,1)}, bf16[384,512]{1,0:T(8,128)(2,1)}, bf16[384,256]{1,0:T(8,128)(2,1)}) custom-call(bf16[384,2048]{1,0:T(8,128)(2,1)} %all-gather.9.cloned.1.call-done.tokens_ref, f32[1,2048]{1,0:T(1,128)} %bitcast.43, bf16[2048,1280]{1,0:T(8,128)(2,1)} %all-gather.11.cloned.1.call-done.weight_ref, ...), custom_call_target="tpu_custom_call" | custom-call | flops 2013265920 | bytes 8388608 | tf_op jit(solution)/shard_map/project/pallas_call | solution.py:186
  122.3 0.0 all-gather.15.cloned.1.call-update
  122.3 0.0 all-gather.13.cloned.1.call-start
  122.3 0.2 copy.17
  122.6 0.0 copy-start.7
  122.6 0.8 constant_dynamic-slice_fusion
  123.5 0.0 all-gather.13.cloned.1.call-update
  123.5 0.0 all-gather.19.cloned.1.call-start
  123.5 0.7 dynamic-slice_bitcast_fusion
  124.3 0.0 all-gather.19.cloned.1.call-update
  124.3 0.0 all-gather.17.cloned.1.call-start
  124.4 1.3 collective-permute-start
  125.7 15.4 %all-gather.1.gates_ref = f32[4,4,384]{2,1,0:T(4,128)} all-gather(f32[1,4,384]{2,1,0:T(4,128)S(1)} %bitcast.40), channel_id=2, replica_groups=mesh['grp'=2,'sp'=4,'tp'=4] {'sp'}, dimensions={0}, use_global_device_ids=true | all-gather | bytes 30720 | tf_op jit(solution)/shard_map/all_gather | solution.py:200
  141.1 0.0 collective-permute-done
  141.1 0.7 pad_maximum_fusion.wkv_ref
  141.8 15.9 %all-gather.15.cloned.1.call-done.kv_ref = bf16[1536,512]{1,0:T(8,128)(2,1)} async-done(((bf16[384,512]{1,0:T(8,128)(2,1)}), bf16[1536,512]{1,0:T(8,128)(2,1)}) %all-gather.15.cloned.1.call-update) | async-done | bytes 1572880 | tf_op jit(solution)/shard_map/all_gather | solution.py:199
  157.7 14.8 %attend.1 = bf16[384,512]{1,0:T(8,128)(2,1)} custom-call(bf16[384,512]{1,0:T(8,128)(2,1)} %get-tuple-element.10.q_ref, bf16[1536,512]{1,0:T(8,128)(2,1)} %all-gather.15.cloned.1.call-done.kv_ref, f32[4,4,384]{2,1,0:T(4,128)} %all-gather.1.gates_ref, bf16[512,256]{1,0:T(8,128)(2,1)} %pad_maximum_fusion.wkv_ref, f32[1,4]{1,0:T(1,128)} %bitcast.44), custom_call_target="tpu_custom_call" | custom-call | flops 1207959552 | bytes 4194304 | tf_op jit(solution)/shard_map/attend/pallas_call | solution.py:201
  172.5 1.8 copy.19
  174.3 0.0 all-gather.17.cloned.1.call-update
  174.3 57.6 %all-gather.13.cloned.1.call-done = bf16[2048,1024]{1,0:T(8,128)(2,1)} async-done(((bf16[256,1024]{1,0:T(8,128)(2,1)}), bf16[2048,1024]{1,0:T(8,128)(2,1)}) %all-gather.13.cloned.1.call-update) | async-done | bytes 4194320 | tf_op jit(solution)/shard_map/all_gather | solution.py:140
  231.9 4.6 %add_divide_fusion = f32[384,1024]{1,0:T(8,128)S(1)} fusion(bf16[384,2048]{1,0:T(8,128)(2,1)} %get-tuple-element.9, bf16[2048,1024]{1,0:T(8,128)(2,1)} %all-gather.13.cloned.1.call-done), kind=kOutput, calls=%fused_computation | convolution fusion | flops 1611792384 | bytes 7340032 | tf_op jit(solution)/shard_map/dot_general | solution.py:213
  236.5 45.1 %all-gather.19.cloned.1.call-done = bf16[1024,2,512]{2,0,1:T(8,128)(2,1)} async-done(((bf16[128,2,512]{2,0,1:T(8,128)(2,1)}), bf16[1024,2,512]{2,0,1:T(8,128)(2,1)}) %all-gather.19.cloned.1.call-update) | async-done | bytes 2097168 | tf_op jit(solution)/shard_map/all_gather | solution.py:140
  281.6 21.3 %all-gather.17.cloned.1.call-done = bf16[384,2,1024]{2,0,1:T(8,128)(2,1)} async-done(((bf16[384,2,256]{2,0,1:T(8,128)(2,1)}), bf16[384,2,1024]{2,0,1:T(8,128)(2,1)}) %all-gather.17.cloned.1.call-update) | async-done | bytes 1572880 | tf_op jit(solution)/shard_map/all_gather | solution.py:216
  302.8 2.2 convolution_multiply_fusion
  305.0 0.0 copy-done.9
  305.0 2.5 fusion.1
  (28 shorter events, 0.2 us)
Async XLA Ops:
  6.5 117.0 %copy-start = (bf16[2,256,512]{2,1,0:T(8,128)(2,1)S(1)}, bf16[2,256,512]{2,1,0:T(8,128)(2,1)}, u32[]{:S(2)}) copy-start(bf16[2,256,512]{2,1,0:T(8,128)(2,1)} %param.25) | copy-start | bytes 1572868
  6.5 2.7 copy-start.3
  6.5 2.8 copy-start.4
  6.5 2.8 copy-start.5
  6.5 2.9 copy-start.6
  6.5 23.0 %all-gather.9.cloned.1.call-start = ((), (), s32[]{:S(2)}) async-start(), calls=%async_computation | async-start | bytes 1966080 | tf_op jit(solution)/shard_map/all_gather | solution.py:163
  7.3 108.6 %all-gather.11.cloned.1.call-start = ((), (), s32[]{:S(2)}) async-start(), calls=%async_computation.1 | async-start | bytes 5898240 | tf_op jit(solution)/shard_map/all_gather | solution.py:140
  9.3 1.1 copy-start.8
  10.4 147.4 %all-gather.15.cloned.1.call-start = ((), (), s32[]{:S(2)}) async-start(), calls=%async_computation.3 | async-start | bytes 1966080 | tf_op jit(solution)/shard_map/all_gather | solution.py:199
  115.8 6.5 %copy-start.1 = (bf16[512,2,512]{2,1,0:T(2,128)(2,1)S(1)}, bf16[512,2,512]{2,1,0:T(2,128)(2,1)}, u32[]{:S(2)}) copy-start(bf16[512,2,512]{2,1,0:T(2,128)(2,1)} %param.24) | copy-start | bytes 3145732
  122.3 109.6 %all-gather.13.cloned.1.call-start = ((), (), s32[]{:S(2)}) async-start(), calls=%async_computation.2 | async-start | bytes 4718592 | tf_op jit(solution)/shard_map/all_gather | solution.py:140
  122.6 1.8 copy-start.2
  122.6 3.1 copy-start.7
  123.5 158.1 %all-gather.19.cloned.1.call-start = ((), (), s32[]{:S(2)}) async-start(), calls=%async_computation.5 | async-start | bytes 2359296 | tf_op jit(solution)/shard_map/all_gather | solution.py:140
  124.3 178.5 %all-gather.17.cloned.1.call-start = ((), (), s32[]{:S(2)}) async-start(), calls=%async_computation.4 | async-start | bytes 1966080 | tf_op jit(solution)/shard_map/all_gather | solution.py:216
  124.4 16.7 %collective-permute-start = (bf16[128,256]{1,0:T(8,128)(2,1)S(1)}, bf16[128,256]{1,0:T(8,128)(2,1)S(1)}, u32[]{:S(2)}, u32[]{:S(2)}) collective-permute-start(bf16[128,256]{1,0:T(8,128)(2,1)S(1)} %slice.38), channel_id=1, source_target_pairs={{0,4},{4,8},{8,12},{1,5},{5,9},{9,13},{2,6},{6,10},{10,14},{3,7},{... | collective-permute-start | bytes 196616 | tf_op jit(solution)/shard_map/ppermute | solution.py:22
  302.8 2.2 copy-start.9
Sparse Core Ops, SparseCore 0:
  8.9 20.5 all-gather.8
  31.7 84.0 all-gather.10
  122.4 35.2 all-gather.14
  159.7 72.1 all-gather.12
  233.9 47.5 all-gather.18
  283.0 19.8 all-gather.16

commit v2 on v1

v2 whole, which is shorter than its diff:
```python
import functools

import jax
import jax.numpy as jnp
from jax import lax
from jax.experimental import pallas as pl
from jax.experimental.pallas import tpu as pltpu
from jax.sharding import PartitionSpec as P

HEAD = 64
PAIR = 2 * HEAD
WINDOW = 128

epsilon = 1e-06
big_negative = -1e30
MESH = pl.DeviceIdType.MESH
VMEM_LIMIT = 60 * 1024 * 1024


def layer_kernel(
    heads, groups,
    tokens_in, kv_in, q_in, merge_in, branch_in, gates_in, norm_gain, head_gain, sink_ref,
    out_ref,
    tok, normed, w_kv, w_q, w_m0, w_m1, w_br, kv, gates, wkv, queries, win, forg, top_s, total_s, mixed_s, gate_s,
    local_sem, tok_sem, z_send, z_recv, y_send, y_recv, kv_send, kv_recv, gt_send, gt_recv, halo_sem, head_sem,
):
    shards, parts, ways = lax.axis_size("sp"), lax.axis_size("grp"), lax.axis_size("tp")
    s, g, t = lax.axis_index("sp"), lax.axis_index("grp"), lax.axis_index("tp")
    rows, depth = normed.shape
    width = heads * HEAD
    low = lax.broadcasted_iota(jnp.int32, (1, PAIR), 1) < HEAD
    contract = (((1,), (1,)), ((), ()))

    chunks = [w_kv, w_q, w_m0, w_m1, w_br]

    def view(chunk, block, part=None):
        ref = chunks[chunk]
        axis = ref.ndim - 2
        share = ref.shape[axis] // shards
        start, size = block * share, share
        if part is not None:
            size = share // parts
            start = start + part * size
        at = pl.ds(pl.multiple_of(start, size), size)
        return ref.at[at, :] if axis == 0 else ref.at[:, at, :]

    def z_copy(direction, chunk, block, index):
        return pltpu.make_async_remote_copy(
            src_ref=view(chunk, block, g),
            dst_ref=view(chunk, block, g),
            send_sem=z_send.at[direction, chunk, index],
            recv_sem=z_recv.at[direction, chunk, index],
            device_id={"sp": s + 1 if direction == 0 else s - 1},
            device_id_type=MESH,
        )

    def y_copy(direction, chunk, block, index, shift, part):
        return pltpu.make_async_remote_copy(
            src_ref=view(chunk, block, part),
            dst_ref=view(chunk, block, part),
            send_sem=y_send.at[direction, chunk, index, shift - 1],
            recv_sem=y_recv.at[direction, chunk, index, shift - 1],
            device_id={"grp": lax.rem(g + shift, parts)},
            device_id_type=MESH,
        )

    def has_next(direction):
        return s + 1 < shards if direction == 0 else s > 0

    def source(direction, step):
        return s - step if direction == 0 else s + step

    def has_source(direction, step):
        return s >= step if direction == 0 else s + step < shards

    def send_own(chunk):
        for direction in range(2):
            @pl.when(has_next(direction))
            def _():
                z_copy(direction, chunk, s, 0).start()

    def relay(chunk, step):
        for direction in range(2):
            @pl.when(has_source(direction, step))
            def _():
                block = source(direction, step)
                z_copy(direction, chunk, block, step - 1).wait_recv()

                @pl.when(has_next(direction) & (step < shards - 1))
                def _():
                    z_copy(direction, chunk, block, step).start()

                for shift in range(1, parts):
                    y_copy(direction, chunk, block, step - 1, shift, g).start()

    def wait_mirror(chunk):
        @pl.loop(1, shards)
        def _(step):
            for direction in range(2):
                @pl.when(has_source(direction, step))
                def _():
                    for shift in range(1, parts):
                        part = lax.rem(g + parts - shift, parts)
                        y_copy(direction, chunk, source(direction, step), step - 1, shift, part).wait_recv()

    def local(index, src, dst):
        return pltpu.make_async_copy(src, dst, local_sem.at[index])

    locals_ = []
    for index, (array, chunk) in enumerate(((kv_in, 0), (q_in, 1))):
        locals_.append(local(index, array, view(chunk, s)))
    channels = out_ref.shape[1]
    locals_.append(local(2, tokens_in, tok.at[t]))
    locals_.append(local(3, gates_in, gates.at[s]))
    locals_.append(local(4, merge_in.at[:, 0:channels], view(2, s)))
    locals_.append(local(5, merge_in.at[:, channels : 2 * channels], view(3, s)))
    locals_.append(local(6, branch_in, view(4, s)))
    for copy in locals_:
        copy.start()

    barrier = pltpu.get_barrier_semaphore()
    for shift in range(1, ways):
        pl.semaphore_signal(barrier, inc=1, device_id={"tp": lax.rem(t + shift, ways)}, device_id_type=MESH)
    for shift in range(1, parts):
        pl.semaphore_signal(barrier, inc=1, device_id={"grp": lax.rem(g + shift, parts)}, device_id_type=MESH)
    for direction in range(2):
        @pl.when(has_next(direction))
        def _():
            pl.semaphore_signal(
                barrier, inc=1, device_id={"sp": s + 1 if direction == 0 else s - 1}, device_id_type=MESH
            )
    for copy in locals_:
        copy.wait()
    neighbours = jnp.minimum(s, 1) + jnp.minimum(shards - 1 - s, 1)
    pl.semaphore_wait(barrier, ways - 1 + parts - 1 + neighbours)

    def tp_copy(ref, slot, sems, kind, shift):
        return pltpu.make_async_remote_copy(
            src_ref=ref.at[slot],
            dst_ref=ref.at[slot],
            send_sem=sems.at[kind, 0, shift - 1],
            recv_sem=sems.at[kind, 1, shift - 1],
            device_id={"tp": lax.rem(t + shift, ways)},
            device_id_type=MESH,
        )

    def tp_send(ref, sems, kind):
        for shift in range(1, ways):
            tp_copy(ref, t, sems, kind, shift).start()

    def tp_wait(ref, sems, kind):
        for shift in range(1, ways):
            tp_copy(ref, lax.rem(t + ways - shift, ways), sems, kind, shift).wait_recv()

    def gates_copy(block, index):
        return pltpu.make_async_remote_copy(
            src_ref=gates.at[block], dst_ref=gates.at[block],
            send_sem=gt_send.at[index], recv_sem=gt_recv.at[index],
            device_id={"sp": s + 1}, device_id_type=MESH,
        )

    def kv_copy(block, index):
        return pltpu.make_async_remote_copy(
            src_ref=kv.at[block], dst_ref=kv.at[block],
            send_sem=kv_send.at[index], recv_sem=kv_recv.at[index],
            device_id={"sp": s + 1}, device_id_type=MESH,
        )

    halo = pltpu.make_async_remote_copy(
        src_ref=wkv.at[pl.ds(rows, WINDOW), :], dst_ref=wkv.at[pl.ds(0, WINDOW), :],
        send_sem=halo_sem.at[0], recv_sem=halo_sem.at[1],
        device_id={"sp": s + 1}, device_id_type=MESH,
    )

    tp_send(tok, tok_sem, 0)
    send_own(0)
    send_own(1)

    @pl.when(has_next(0))
    def _():
        gates_copy(s, 0).start()

    tp_wait(tok, tok_sem, 0)
    share = depth // ways
    squares = jnp.zeros((rows, 1), jnp.float32)
    for way in range(ways):
        x = tok[way].astype(jnp.float32)
        squares = squares + jnp.sum(x * x, axis=-1, keepdims=True)
    scale = lax.rsqrt(squares * (1.0 / depth) + epsilon)
    for way in range(ways):
        at = slice(way * share, (way + 1) * share)
        normed[:, at] = (tok[way].astype(jnp.float32) * scale * norm_gain[:, at]).astype(jnp.bfloat16)

    @pl.loop(1, shards)
    def _(step):
        @pl.when(step == shards - 1)
        def _():
            send_own(2)

        relay(0, step)
        relay(1, step)

    def project(weight_ref, offset, width, flags, gain_at, store):
        raw = jnp.dot(normed[...], weight_ref[:, offset : offset + width], preferred_element_type=jnp.float32)
        for at in range(0, width, PAIR):
            part = raw[:, at : at + PAIR]
            first, second = flags[at // HEAD], flags[at // HEAD + 1]
            if first or second:
                power = part * part
                lower = jnp.sum(jnp.where(low, power, 0.0), axis=-1, keepdims=True)
                upper = jnp.sum(jnp.where(low, 0.0, power), axis=-1, keepdims=True)
                factor = jnp.where(
                    low,
                    lax.rsqrt(lower * (1.0 / HEAD) + epsilon),
                    lax.rsqrt(upper * (1.0 / HEAD) + epsilon),
                )
                scaled = part * factor * head_gain[:, gain_at + at : gain_at + at + PAIR]
                part = scaled if first and second else jnp.where(low if first else ~low, scaled, part)
            store(at, part.astype(jnp.bfloat16))

    def store_wkv(at, value):
        wkv[WINDOW : WINDOW + rows, at : at + PAIR] = value

    def store_kv(at, value):
        kv[s, :, at : at + PAIR] = value

    def store_q(at, value):
        queries[:, at : at + PAIR] = value * jnp.bfloat16(HEAD ** -0.5)

    small = 2 * groups * HEAD
    wait_mirror(0)
    project(w_kv, 2 * width, small, (True,) * groups + (False,) * groups, 2 * width, store_wkv)
    project(w_kv, 0, 2 * width, (True,) * heads + (False,) * heads, 0, store_kv)
    wait_mirror(1)
    project(w_q, 0, 2 * width, (True,) * (2 * heads), 2 * width + small, store_q)

    @pl.when(has_next(0))
    def _():
        halo.start()
        kv_copy(s, 0).start()

    @pl.when(s == 0)
    def _():
        wkv[0:WINDOW, :] = jnp.zeros((WINDOW, small), jnp.bfloat16)

    diagonal = lax.broadcasted_iota(jnp.int32, (rows, rows), 0) >= lax.broadcasted_iota(
        jnp.int32, (rows, rows), 1
    )

    def absorb(block, first):
        for head in range(heads):
            lanes = head // 2 * PAIR
            pick = low if head % 2 == 0 else ~low
            mine = jnp.where(pick, queries[:, width + lanes : width + lanes + PAIR], jnp.bfloat16(0))
            keys = kv[block, :, lanes : lanes + PAIR]
            values = kv[block, :, width + lanes : width + lanes + PAIR]
            scores = lax.dot_general(mine, keys, contract, preferred_element_type=jnp.float32)
            scores = scores - gates[block, head : head + 1, :]
            if first:
                scores = jnp.where(diagonal, scores, big_negative)
                top = jnp.max(scores, axis=-1, keepdims=True)
                weights = jnp.where(diagonal, jnp.exp(scores - top), 0.0)
            else:
                old = top_s[head, :, 0:1]
                top = jnp.maximum(old, jnp.max(scores, axis=-1, keepdims=True))
                weights = jnp.exp(scores - top)
            total = jnp.sum(weights, axis=-1, keepdims=True)
            mixed = jnp.dot(weights.astype(jnp.bfloat16), values, preferred_element_type=jnp.float32)
            if not first:
                shrink = jnp.exp(old - top)
                total = total + total_s[head, :, 0:1] * shrink
                mixed = mixed + mixed_s[head] * shrink
            top_s[head, :, 0:1] = top
            total_s[head, :, 0:1] = total
            mixed_s[head] = mixed

    absorb(s, True)

    @pl.when(s > 0)
    def _():
        halo.wait_recv()

    for pair in range(heads // 2):
        lanes = pair * PAIR
        keys = wkv[:, pair * HEAD : (pair + 1) * HEAD]
        values = wkv[:, groups * HEAD + pair * HEAD : groups * HEAD + (pair + 1) * HEAD]
        keys = jnp.concatenate([keys, keys], axis=1)
        values = jnp.concatenate([values, values], axis=1)
        row_at = lax.broadcasted_iota(jnp.int32, (WINDOW, 2 * WINDOW), 0)
        col_at = lax.broadcasted_iota(jnp.int32, (WINDOW, 2 * WINDOW), 1)
        inside = (col_at > row_at) & (col_at <= row_at + WINDOW)
        for at in range(0, rows, WINDOW):
            near_queries = queries[at : at + WINDOW, lanes : lanes + PAIR]
            near, near_values = keys[at : at + 2 * WINDOW], values[at : at + 2 * WINDOW]
            valid = inside & ((col_at >= WINDOW) | (s > 0)) if at == 0 else inside
            results = []
            for half in range(2):
                head = pair * 2 + half
                mine = jnp.where(low if half == 0 else ~low, near_queries, jnp.bfloat16(0))
                scores = lax.dot_general(mine, near, contract, preferred_element_type=jnp.float32)
                sink = sink_ref[:, head : head + 1]
                top = jnp.maximum(
                    jnp.max(jnp.where(valid, scores, big_negative), axis=-1, keepdims=True), sink
                )
                weights = jnp.where(valid, jnp.exp(scores - top), 0.0)
                total = jnp.sum(weights, axis=-1, keepdims=True) + jnp.exp(sink - top)
                probs = (weights / total).astype(jnp.bfloat16)
                results.append(jnp.dot(probs, near_values, preferred_element_type=jnp.float32))
            win[t, at : at + WINDOW, lanes : lanes + PAIR] = jnp.where(low, results[0], results[1]).astype(
                jnp.bfloat16
            )

    @pl.loop(1, shards + 2)
    def _(wave):
        @pl.when(wave == 1)
        def _():
            send_own(3)
            tp_send(win, head_sem, 0)

        @pl.when(wave == 2)
        def _():
            send_own(4)

        @pl.when(s >= wave)
        def _():
            gates_copy(s - wave, wave - 1).wait_recv()
            kv_copy(s - wave, wave - 1).wait_recv()

            @pl.when(has_next(0))
            def _():
                gates_copy(s - wave, wave).start()
                kv_copy(s - wave, wave).start()

        for offset in range(3):
            step = wave - offset

            @pl.when((step >= 1) & (step < shards))
            def _():
                relay(2 + offset, step)

        @pl.when(s >= wave)
        def _():
            absorb(s - wave, False)

        @pl.when(wave == FORGET_DONE(shards))
        def _():
            for pair in range(heads // 2):
                even, odd = 2 * pair, 2 * pair + 1
                mixed = jnp.where(
                    low, mixed_s[even] / total_s[even, :, 0:1], mixed_s[odd] / total_s[odd, :, 0:1]
                )
                forg[t, :, pair * PAIR : (pair + 1) * PAIR] = mixed.astype(jnp.bfloat16)
            tp_send(forg, head_sem, 1)

    wait_mirror(2)
    gate_s[0] = jax.nn.sigmoid(jnp.dot(normed[...], w_m0[...], preferred_element_type=jnp.float32))
    wait_mirror(3)
    gate_s[1] = jax.nn.sigmoid(jnp.dot(normed[...], w_m1[...], preferred_element_type=jnp.float32))
    tp_wait(win, head_sem, 0)
    tp_wait(forg, head_sem, 1)
    wait_mirror(4)
    total = None
    for branch, ref in enumerate((win, forg)):
        projection = None
        for way in range(ways):
            term = jnp.dot(
                ref[way], w_br[branch, way * width : (way + 1) * width, :], preferred_element_type=jnp.float32
            )
            projection = term if projection is None else projection + term
        gated = gate_s[branch] * projection
        total = gated if total is None else total + gated
    out_ref[...] = total.astype(jnp.bfloat16)

    for shift in range(1, ways):
        tp_copy(tok, t, tok_sem, 0, shift).wait_send()
        tp_copy(win, t, head_sem, 0, shift).wait_send()
        tp_copy(forg, t, head_sem, 1, shift).wait_send()

    @pl.when(has_next(0))
    def _():
        halo.wait_send()

    @pl.loop(0, shards)
    def _(step):
        @pl.when(has_next(0) & (s >= step))
        def _():
            kv_copy(s - step, step).wait_send()
            gates_copy(s - step, step).wait_send()

        for chunk in range(len(chunks)):
            for direction in range(2):
                @pl.when(has_next(direction) & has_source(direction, step))
                def _():
                    z_copy(direction, chunk, source(direction, step), step).wait_send()

                @pl.when((step >= 1) & has_source(direction, step))
                def _():
                    for shift in range(1, parts):
                        y_copy(direction, chunk, source(direction, step), step - 1, shift, g).wait_send()


def FORGET_DONE(shards):
    return max(shards - 1, 1)


def on_device(
    tokens,
    norm_gain,
    qk_gain,
    w_query_window,
    w_key_window,
    w_value_window,
    sink_logits,
    w_query_forget,
    w_key_forget,
    w_value_forget,
    gate_cum,
    w_merge,
    w_branch,
):
    rows, share = tokens.shape
    shards, parts, ways = lax.axis_size("sp"), lax.axis_size("grp"), lax.axis_size("tp")
    heads = w_query_window.shape[1] // HEAD
    groups = w_key_window.shape[1] // HEAD
    channels = w_merge.shape[2]
    depth, width, small = share * ways, heads * HEAD, 2 * groups * HEAD
    kv_in = jnp.concatenate([w_key_forget, w_value_forget, w_key_window, w_value_window], axis=1)
    q_in = jnp.concatenate([w_query_window, w_query_forget], axis=1)
    head_gains = jnp.concatenate(
        [
            jnp.tile(qk_gain[3], heads),
            jnp.ones((width,), jnp.float32),
            jnp.tile(qk_gain[1], groups),
            jnp.ones((groups * HEAD,), jnp.float32),
            jnp.tile(qk_gain[0], heads),
            jnp.tile(qk_gain[2], heads),
        ]
    )[None]
    half = jnp.bfloat16
    dma = pltpu.SemaphoreType.DMA
    anywhere, inside = pl.BlockSpec(memory_space=pl.ANY), pl.BlockSpec(memory_space=pltpu.VMEM)
    return pl.pallas_call(
        functools.partial(layer_kernel, heads, groups),
        out_shape=jax.ShapeDtypeStruct((rows, channels), half),
        in_specs=[anywhere] * 6 + [inside] * 3,
        out_specs=inside,
        scratch_shapes=[
            pltpu.VMEM((ways, rows, share), half),
            pltpu.VMEM((rows, depth), half),
            pltpu.VMEM((depth, 2 * width + small), half),
            pltpu.VMEM((depth, 2 * width), half),
            pltpu.VMEM((depth, channels), half),
            pltpu.VMEM((depth, channels), half),
            pltpu.VMEM((2, ways * width, channels), half),
            pltpu.VMEM((shards, rows, 2 * width), half),
            pltpu.VMEM((shards, heads, rows), jnp.float32),
            pltpu.VMEM((rows + WINDOW, small), half),
            pltpu.VMEM((rows, 2 * width), half),
            pltpu.VMEM((ways, rows, width), half),
            pltpu.VMEM((ways, rows, width), half),
            pltpu.VMEM((heads, rows, 128), jnp.float32),
            pltpu.VMEM((heads, rows, 128), jnp.float32),
            pltpu.VMEM((heads, rows, PAIR), jnp.float32),
            pltpu.VMEM((2, rows, channels), jnp.float32),
            dma((7,)),
            dma((1, 2, ways - 1)),
            dma((2, 5, shards)),
            dma((2, 5, shards)),
            dma((2, 5, shards, parts - 1)),
            dma((2, 5, shards, parts - 1)),
            dma((shards,)),
            dma((shards,)),
            dma((shards,)),
            dma((shards,)),
            dma((2,)),
            dma((2, 2, ways - 1)),
        ],
        compiler_params=pltpu.CompilerParams(
            collective_id=0, has_side_effects=True, vmem_limit_bytes=VMEM_LIMIT
        ),
        name="layer",
    )(
        tokens, kv_in, q_in, w_merge.reshape(w_merge.shape[0], -1), w_branch, gate_cum.T,
        norm_gain[None], head_gains, sink_logits[None],
    )


def solution(mesh):
    return jax.shard_map(
        on_device,
        mesh=mesh,
        in_specs=(
            P(("grp", "sp"), "tp"),
            P(),
            P(),
            P("sp", "tp"),
            P("sp", "tp"),
            P("sp", "tp"),
            P("tp"),
            P("sp", "tp"),
            P("sp", "tp"),
            P("sp", "tp"),
            P(("grp", "sp"), "tp"),
            P("sp", None, "tp"),
            P(None, "sp", "tp"),
        ),
        out_specs=P(("grp", "sp"), "tp"),
        check_vma=False,
    )
```

time: 316 us -> 153 us (0.48)
  the two profiles are of different devices: /device:TPU:24 before, /device:TPU:29 now
where the time goes in v2:
time: 153 us
  Pallas kernels  145 us (95%)
  local copies, waits for them, and re-layouts  5.34 us (3%)
  other arithmetic  2.86 us (2%)
    pallas_call x1, Pallas kernels, on_device(): pl.pallas_call(functools.partial(layer_kernel, heads, groups), out_shape=...  145 us
    unnamed x17, local copies, waits for them, and re-layouts  3.56 us

profile of v2, /device:TPU:29, one launch (start us, length us, event | category | flops | bytes accessed | tf_op | source)
XLA Modules:
  0.0 152.9 jit_solution(3638028773248283788)
XLA Ops:
  0.0 0.0 copy-start.1
  0.0 0.0 copy-start.2
  0.0 0.0 copy-start.3
  0.0 0.0 copy-start.4
  0.0 0.8 slice_bitcast_fusion
  0.9 0.1 tile.45
  0.9 0.1 tile.51
  1.0 0.1 tile.42
  1.1 0.1 tile.48
  1.3 0.6 broadcast_in_dim.18.head_gain
  1.9 1.9 %pad_maximum_fusion.1.q_in = bf16[512,512]{1,0:T(8,128)(2,1)} fusion(bf16[512,256]{1,0:T(8,128)(2,1)} %param.20, bf16[512,256]{1,0:T(8,128)(2,1)} %param.16), kind=kLoop, calls=%fused_computation.1 | loop fusion | flops 1048576 | bytes 1048576 | tf_op jit(solution)/shard_map/concatenate | solution.py:428
  3.7 0.0 copy-done.1
  3.8 0.0 copy-done.2
  3.8 0.0 copy-done.3
  3.8 0.0 copy-done.4
  3.8 0.0 copy-start
  3.8 1.0 pad_maximum_fusion.kv_in
  4.8 0.5 copy-done
  5.3 1.2 copy.14
  6.5 144.6 %layer.1 = bf16[384,512]{1,0:T(8,128)(2,1)} custom-call(bf16[384,512]{1,0:T(8,128)(2,1)} %tokens_in.1, bf16[512,768]{1,0:T(8,128)(2,1)} %pad_maximum_fusion.kv_in, bf16[512,512]{1,0:T(8,128)(2,1)} %pad_maximum_fusion.1.q_in, bf16[512,1024]{1,0:T(8,128)(2,1)} %bitcast.13, bf16[2,256,512]{2,1,0:T(8,128)(2,1)} %branch_in.1, f32[4,384]{1,0:T(4,128)} %bitcast.16, ...), custom_call_target="tpu_custom_call" | custom-call | tf_op jit(solution)/shard_map/layer/pallas_call | solution.py:442
  151.1 1.8 %copy.22 = bf16[384,512]{1,0:T(8,128)(2,1)} copy(bf16[384,512]{1,0:T(8,128)(2,1)} %layer.1) | data formatting | bytes 786432
  (11 shorter events, 0.0 us)
Async XLA Ops:
  0.0 3.8 %copy-start.1 = (bf16[512,256]{1,0:T(8,128)(2,1)S(1)}, bf16[512,256]{1,0:T(8,128)(2,1)}, u32[]{:S(2)}) copy-start(bf16[512,256]{1,0:T(8,128)(2,1)} %param.22) | copy-start | bytes 786436
  0.0 3.8 %copy-start.2 = (bf16[512,256]{1,0:T(8,128)(2,1)S(1)}, bf16[512,256]{1,0:T(8,128)(2,1)}, u32[]{:S(2)}) copy-start(bf16[512,256]{1,0:T(8,128)(2,1)} %param.21) | copy-start | bytes 786436
  0.0 3.8 %copy-start.3 = (bf16[512,128]{1,0:T(8,128)(2,1)S(1)}, bf16[512,128]{1,0:T(8,128)(2,1)}, u32[]{:S(2)}) copy-start(bf16[512,128]{1,0:T(8,128)(2,1)} %param.18) | copy-start | bytes 393220
  0.0 3.8 %copy-start.4 = (bf16[512,128]{1,0:T(8,128)(2,1)S(1)}, bf16[512,128]{1,0:T(8,128)(2,1)}, u32[]{:S(2)}) copy-start(bf16[512,128]{1,0:T(8,128)(2,1)} %param.17) | copy-start | bytes 393220
  3.8 1.5 copy-start

commit v3 on v2

--- a/solution.py
+++ b/solution.py
@@ -19,9 +19,9 @@
 
 def layer_kernel(
     heads, groups,
-    tokens_in, kv_in, q_in, merge_in, branch_in, gates_in, norm_gain, head_gain, sink_ref,
+    tokens_in, qw_in, kvw_in, qf_in, kf_in, vf_in, merge_in, branch_in, gates_in, norm_gain, qk_gain, sink_ref,
     out_ref,
-    tok, normed, w_kv, w_q, w_m0, w_m1, w_br, kv, gates, wkv, queries, win, forg, top_s, total_s, mixed_s, gate_s,
+    tok, normed, w_kv, w_q, w_m0, w_m1, w_b0, w_b1, kv, gates, wkv, queries, win, forg, top_s, total_s, mixed_s, gate_s,
     local_sem, tok_sem, z_send, z_recv, y_send, y_recv, kv_send, kv_recv, gt_send, gt_recv, halo_sem, head_sem,
 ):
     shards, parts, ways = lax.axis_size("sp"), lax.axis_size("grp"), lax.axis_size("tp")
@@ -31,7 +31,7 @@
     low = lax.broadcasted_iota(jnp.int32, (1, PAIR), 1) < HEAD
     contract = (((1,), (1,)), ((), ()))
 
-    chunks = [w_kv, w_q, w_m0, w_m1, w_br]
+    chunks = [w_kv, w_q, w_m0, w_m1, w_b0, w_b1]
 
     def view(chunk, block, part=None):
         ref = chunks[chunk]
@@ -106,15 +106,23 @@
     def local(index, src, dst):
         return pltpu.make_async_copy(src, dst, local_sem.at[index])
 
-    locals_ = []
-    for index, (array, chunk) in enumerate(((kv_in, 0), (q_in, 1))):
-        locals_.append(local(index, array, view(chunk, s)))
     channels = out_ref.shape[1]
-    locals_.append(local(2, tokens_in, tok.at[t]))
-    locals_.append(local(3, gates_in, gates.at[s]))
-    locals_.append(local(4, merge_in.at[:, 0:channels], view(2, s)))
-    locals_.append(local(5, merge_in.at[:, channels : 2 * channels], view(3, s)))
-    locals_.append(local(6, branch_in, view(4, s)))
+    small = 2 * groups * HEAD
+    pieces = [
+        (tokens_in, tok.at[t]),
+        (gates_in, gates.at[s]),
+        (merge_in.at[:, 0:channels], view(2, s)),
+        (merge_in.at[:, channels : 2 * channels], view(3, s)),
+        (branch_in.at[0], view(4, s)),
+        (branch_in.at[1], view(5, s)),
+    ]
+    for chunk, arrays in ((0, (kf_in, vf_in, kvw_in)), (1, (qw_in, qf_in))):
+        start = 0
+        for array in arrays:
+            size = array.shape[1]
+            pieces.append((array, view(chunk, s).at[:, start : start + size]))
+            start += size
+    locals_ = [local(index, src, dst) for index, (src, dst) in enumerate(pieces)]
     for copy in locals_:
         copy.start()
 
@@ -180,32 +188,31 @@
     def _():
         gates_copy(s, 0).start()
 
-    tp_wait(tok, tok_sem, 0)
-    share = depth // ways
-    squares = jnp.zeros((rows, 1), jnp.float32)
-    for way in range(ways):
-        x = tok[way].astype(jnp.float32)
-        squares = squares + jnp.sum(x * x, axis=-1, keepdims=True)
-    scale = lax.rsqrt(squares * (1.0 / depth) + epsilon)
-    for way in range(ways):
-        at = slice(way * share, (way + 1) * share)
-        normed[:, at] = (tok[way].astype(jnp.float32) * scale * norm_gain[:, at]).astype(jnp.bfloat16)
-
     @pl.loop(1, shards)
     def _(step):
         @pl.when(step == shards - 1)
         def _():
             send_own(2)
+            tp_wait(tok, tok_sem, 0)
+            share = depth // ways
+            squares = jnp.zeros((rows, 1), jnp.float32)
+            for way in range(ways):
+                x = tok[way].astype(jnp.float32)
+                squares = squares + jnp.sum(x * x, axis=-1, keepdims=True)
+            scale = lax.rsqrt(squares * (1.0 / depth) + epsilon)
+            for way in range(ways):
+                at = slice(way * share, (way + 1) * share)
+                normed[:, at] = (tok[way].astype(jnp.float32) * scale * norm_gain[:, at]).astype(jnp.bfloat16)
 
         relay(0, step)
         relay(1, step)
 
-    def project(weight_ref, offset, width, flags, gain_at, store):
+    def project(weight_ref, offset, width, flags, store):
         raw = jnp.dot(normed[...], weight_ref[:, offset : offset + width], preferred_element_type=jnp.float32)
         for at in range(0, width, PAIR):
             part = raw[:, at : at + PAIR]
             first, second = flags[at // HEAD], flags[at // HEAD + 1]
-            if first or second:
+            if first is not None or second is not None:
                 power = part * part
                 lower = jnp.sum(jnp.where(low, power, 0.0), axis=-1, keepdims=True)
                 upper = jnp.sum(jnp.where(low, 0.0, power), axis=-1, keepdims=True)
@@ -214,8 +221,11 @@
                     lax.rsqrt(lower * (1.0 / HEAD) + epsilon),
                     lax.rsqrt(upper * (1.0 / HEAD) + epsilon),
                 )
-                scaled = part * factor * head_gain[:, gain_at + at : gain_at + at + PAIR]
-                part = scaled if first and second else jnp.where(low if first else ~low, scaled, part)
+                gain = jnp.concatenate([qk_gain[k : k + 1, :] for k in (first or 0, second or 0)], axis=1)
+                scaled = part * factor * gain
+                if first is None or second is None:
+                    scaled = jnp.where(~low if first is None else low, scaled, part)
+                part = scaled
             store(at, part.astype(jnp.bfloat16))
 
     def store_wkv(at, value):
@@ -227,12 +237,11 @@
     def store_q(at, value):
         queries[:, at : at + PAIR] = value * jnp.bfloat16(HEAD ** -0.5)
 
-    small = 2 * groups * HEAD
     wait_mirror(0)
-    project(w_kv, 2 * width, small, (True,) * groups + (False,) * groups, 2 * width, store_wkv)
-    project(w_kv, 0, 2 * width, (True,) * heads + (False,) * heads, 0, store_kv)
+    project(w_kv, 2 * width, small, (1,) * groups + (None,) * groups, store_wkv)
+    project(w_kv, 0, 2 * width, (3,) * heads + (None,) * heads, store_kv)
     wait_mirror(1)
-    project(w_q, 0, 2 * width, (True,) * (2 * heads), 2 * width + small, store_q)
+    project(w_q, 0, 2 * width, (0,) * heads + (2,) * heads, store_q)
 
     @pl.when(has_next(0))
     def _():
@@ -310,8 +319,13 @@
                 jnp.bfloat16
             )
 
-    @pl.loop(1, shards + 2)
+    @pl.loop(1, shards + 3)
     def _(wave):
+        @pl.when(wave == shards + 1)
+        def _():
+            wait_mirror(2)
+            gate_s[0] = jax.nn.sigmoid(jnp.dot(normed[...], w_m0[...], preferred_element_type=jnp.float32))
+
         @pl.when(wave == 1)
         def _():
             send_own(3)
@@ -320,6 +334,7 @@
         @pl.when(wave == 2)
         def _():
             send_own(4)
+            send_own(5)
 
         @pl.when(s >= wave)
         def _():
@@ -331,7 +346,7 @@
                 gates_copy(s - wave, wave).start()
                 kv_copy(s - wave, wave).start()
 
-        for offset in range(3):
+        for offset in range(4):
             step = wave - offset
 
             @pl.when((step >= 1) & (step < shards))
@@ -352,19 +367,17 @@
                 forg[t, :, pair * PAIR : (pair + 1) * PAIR] = mixed.astype(jnp.bfloat16)
             tp_send(forg, head_sem, 1)
 
-    wait_mirror(2)
-    gate_s[0] = jax.nn.sigmoid(jnp.dot(normed[...], w_m0[...], preferred_element_type=jnp.float32))
     wait_mirror(3)
     gate_s[1] = jax.nn.sigmoid(jnp.dot(normed[...], w_m1[...], preferred_element_type=jnp.float32))
     tp_wait(win, head_sem, 0)
     tp_wait(forg, head_sem, 1)
-    wait_mirror(4)
     total = None
-    for branch, ref in enumerate((win, forg)):
+    for branch, (ref, w_out) in enumerate(((win, w_b0), (forg, w_b1))):
+        wait_mirror(4 + branch)
         projection = None
         for way in range(ways):
             term = jnp.dot(
-                ref[way], w_br[branch, way * width : (way + 1) * width, :], preferred_element_type=jnp.float32
+                ref[way], w_out[way * width : (way + 1) * width, :], preferred_element_type=jnp.float32
             )
             projection = term if projection is None else projection + term
         gated = gate_s[branch] * projection
@@ -424,25 +437,13 @@
     groups = w_key_window.shape[1] // HEAD
     channels = w_merge.shape[2]
     depth, width, small = share * ways, heads * HEAD, 2 * groups * HEAD
-    kv_in = jnp.concatenate([w_key_forget, w_value_forget, w_key_window, w_value_window], axis=1)
-    q_in = jnp.concatenate([w_query_window, w_query_forget], axis=1)
-    head_gains = jnp.concatenate(
-        [
-            jnp.tile(qk_gain[3], heads),
-            jnp.ones((width,), jnp.float32),
-            jnp.tile(qk_gain[1], groups),
-            jnp.ones((groups * HEAD,), jnp.float32),
-            jnp.tile(qk_gain[0], heads),
-            jnp.tile(qk_gain[2], heads),
-        ]
-    )[None]
     half = jnp.bfloat16
     dma = pltpu.SemaphoreType.DMA
     anywhere, inside = pl.BlockSpec(memory_space=pl.ANY), pl.BlockSpec(memory_space=pltpu.VMEM)
     return pl.pallas_call(
         functools.partial(layer_kernel, heads, groups),
         out_shape=jax.ShapeDtypeStruct((rows, channels), half),
-        in_specs=[anywhere] * 6 + [inside] * 3,
+        in_specs=[anywhere] * 9 + [inside] * 3,
         out_specs=inside,
         scratch_shapes=[
             pltpu.VMEM((ways, rows, share), half),
@@ -451,7 +452,8 @@
             pltpu.VMEM((depth, 2 * width), half),
             pltpu.VMEM((depth, channels), half),
             pltpu.VMEM((depth, channels), half),
-            pltpu.VMEM((2, ways * width, channels), half),
+            pltpu.VMEM((ways * width, channels), half),
+            pltpu.VMEM((ways * width, channels), half),
             pltpu.VMEM((shards, rows, 2 * width), half),
             pltpu.VMEM((shards, heads, rows), jnp.float32),
             pltpu.VMEM((rows + WINDOW, small), half),
@@ -462,12 +464,12 @@
             pltpu.VMEM((heads, rows, 128), jnp.float32),
             pltpu.VMEM((heads, rows, PAIR), jnp.float32),
             pltpu.VMEM((2, rows, channels), jnp.float32),
-            dma((7,)),
+            dma((11,)),
             dma((1, 2, ways - 1)),
-            dma((2, 5, shards)),
-            dma((2, 5, shards)),
-            dma((2, 5, shards, parts - 1)),
-            dma((2, 5, shards, parts - 1)),
+            dma((2, 6, shards)),
+            dma((2, 6, shards)),
+            dma((2, 6, shards, parts - 1)),
+            dma((2, 6, shards, parts - 1)),
             dma((shards,)),
             dma((shards,)),
             dma((shards,)),
@@ -480,8 +482,8 @@
         ),
         name="layer",
     )(
-        tokens, kv_in, q_in, w_merge.reshape(w_merge.shape[0], -1), w_branch, gate_cum.T,
-        norm_gain[None], head_gains, sink_logits[None],
+        tokens, w_query_window, jnp.concatenate([w_key_window, w_value_window], axis=1), w_query_forget, w_key_forget, w_value_forget,
+        w_merge.reshape(w_merge.shape[0], -1), w_branch, gate_cum.T, norm_gain[None], qk_gain, sink_logits[None],
     )
 
 

time: 153 us -> 151 us (0.987)
  the two profiles are of different devices: /device:TPU:29 before, /device:TPU:24 now
where the time goes in v3:
time: 151 us
  Pallas kernels  145 us (96%)
  local copies, waits for them, and re-layouts  4.23 us (3%)
  other arithmetic  1.7 us (1%)
    pallas_call x1, Pallas kernels, on_device(): pl.pallas_call(functools.partial(layer_kernel, heads, groups), out_shape=...  145 us
    unnamed x2, local copies, waits for them, and re-layouts  4.23 us

profile of v3, /device:TPU:24, one launch (start us, length us, event | category | flops | bytes accessed | tf_op | source)
XLA Modules:
  0.0 150.5 jit_solution(9165274691970109667)
XLA Ops:
  0.0 1.7 %pad_maximum_fusion.kvw_in = bf16[512,256]{1,0:T(8,128)(2,1)} fusion(bf16[512,128]{1,0:T(8,128)(2,1)} %param.18, bf16[512,128]{1,0:T(8,128)(2,1)} %param.17), kind=kLoop, calls=%fused_computation | loop fusion | flops 524288 | bytes 524288 | tf_op jit(solution)/shard_map/concatenate | solution.py:485
  1.7 2.5 %copy.14 = bf16[64,8,2,512]{3,1,2,0:T(8,128)(2,1)} copy(bf16[64,8,2,512]{3,2,1,0:T(2,128)(2,1)} %bitcast.6) | data formatting | bytes 2097152
  4.2 144.6 %layer.1 = bf16[384,512]{1,0:T(8,128)(2,1)} custom-call(bf16[384,512]{1,0:T(8,128)(2,1)} %tokens_in.1, bf16[512,256]{1,0:T(8,128)(2,1)} %qw_in.1, bf16[512,256]{1,0:T(8,128)(2,1)} %pad_maximum_fusion.kvw_in, bf16[512,256]{1,0:T(8,128)(2,1)} %qf_in.1, bf16[512,256]{1,0:T(8,128)(2,1)} %kf_in.1, bf16[512,256]{1,0:T(8,128)(2,1)} %vf_in.1, ...), custom_call_target="tpu_custom_call" | custom-call | tf_op jit(solution)/shard_map/layer/pallas_call | solution.py:443
  148.8 1.8 %copy.16 = bf16[384,512]{1,0:T(8,128)(2,1)} copy(bf16[384,512]{1,0:T(8,128)(2,1)} %layer.1) | data formatting | bytes 786432

commit v4 on v3

--- a/solution.py
+++ b/solution.py
@@ -319,22 +319,14 @@
                 jnp.bfloat16
             )
 
-    @pl.loop(1, shards + 3)
+    @pl.loop(1, shards)
     def _(wave):
-        @pl.when(wave == shards + 1)
-        def _():
-            wait_mirror(2)
-            gate_s[0] = jax.nn.sigmoid(jnp.dot(normed[...], w_m0[...], preferred_element_type=jnp.float32))
-
         @pl.when(wave == 1)
         def _():
             send_own(3)
-            tp_send(win, head_sem, 0)
-
-        @pl.when(wave == 2)
-        def _():
             send_own(4)
             send_own(5)
+            tp_send(win, head_sem, 0)
 
         @pl.when(s >= wave)
         def _():
@@ -345,13 +337,6 @@
             def _():
                 gates_copy(s - wave, wave).start()
                 kv_copy(s - wave, wave).start()
-
-        for offset in range(4):
-            step = wave - offset
-
-            @pl.when((step >= 1) & (step < shards))
-            def _():
-                relay(2 + offset, step)
 
         @pl.when(s >= wave)
         def _():
@@ -367,6 +352,11 @@
                 forg[t, :, pair * PAIR : (pair + 1) * PAIR] = mixed.astype(jnp.bfloat16)
             tp_send(forg, head_sem, 1)
 
+        for chunk in range(2, len(chunks)):
+            relay(chunk, wave)
+
+    wait_mirror(2)
+    gate_s[0] = jax.nn.sigmoid(jnp.dot(normed[...], w_m0[...], preferred_element_type=jnp.float32))
     wait_mirror(3)
     gate_s[1] = jax.nn.sigmoid(jnp.dot(normed[...], w_m1[...], preferred_element_type=jnp.float32))
     tp_wait(win, head_sem, 0)

time: 151 us -> 145 us (0.960)
  Pallas kernels: 145 us -> 139 us
    pallas_call x1, Pallas kernels: 145 us -> 139 us  [on_device(): pl.pallas_call(functools.partial(layer_kernel, heads, groups), out_shape=...]
where the time goes in v4:
time: 145 us
  Pallas kernels  139 us (96%)
  local copies, waits for them, and re-layouts  4.23 us (3%)
  other arithmetic  1.7 us (1%)
    pallas_call x1, Pallas kernels, on_device(): pl.pallas_call(functools.partial(layer_kernel, heads, groups), out_shape=...  139 us
    unnamed x2, local copies, waits for them, and re-layouts  4.23 us

profile of v4, /device:TPU:24, one launch (start us, length us, event | category | flops | bytes accessed | tf_op | source)
XLA Modules:
  0.0 144.9 jit_solution(17850764466066923741)
XLA Ops:
  0.0 1.7 %pad_maximum_fusion.kvw_in = bf16[512,256]{1,0:T(8,128)(2,1)} fusion(bf16[512,128]{1,0:T(8,128)(2,1)} %param.18, bf16[512,128]{1,0:T(8,128)(2,1)} %param.17), kind=kLoop, calls=%fused_computation | loop fusion | flops 524288 | bytes 524288 | tf_op jit(solution)/shard_map/concatenate | solution.py:475
  1.7 2.5 %copy.14 = bf16[64,8,2,512]{3,1,2,0:T(8,128)(2,1)} copy(bf16[64,8,2,512]{3,2,1,0:T(2,128)(2,1)} %bitcast.6) | data formatting | bytes 2097152
  4.2 139.0 %layer.1 = bf16[384,512]{1,0:T(8,128)(2,1)} custom-call(bf16[384,512]{1,0:T(8,128)(2,1)} %tokens_in.1, bf16[512,256]{1,0:T(8,128)(2,1)} %qw_in.1, bf16[512,256]{1,0:T(8,128)(2,1)} %pad_maximum_fusion.kvw_in, bf16[512,256]{1,0:T(8,128)(2,1)} %qf_in.1, bf16[512,256]{1,0:T(8,128)(2,1)} %kf_in.1, bf16[512,256]{1,0:T(8,128)(2,1)} %vf_in.1, ...), custom_call_target="tpu_custom_call" | custom-call | tf_op jit(solution)/shard_map/layer/pallas_call | solution.py:433
  143.2 1.8 %copy.16 = bf16[384,512]{1,0:T(8,128)(2,1)} copy(bf16[384,512]{1,0:T(8,128)(2,1)} %layer.1) | data formatting | bytes 786432
